TPU v7x, 512 devices: a whole 4x4x16 slice. The times are simulated.
512 devices in a mesh: fs: 64 (over z, y), tp: 8 (over x, core).
Axes of the slice: x: 4, y: 4, z: 16, core: 2. Of those that a mesh axis runs over, the one named last changes fastest.
Arguments:
- tokens: bfloat16 [49152, 2048], P('fs'), may hold values from -6 to 6
- norm_gain: float32 [2048], replicated, may hold values from 0.1 to 1.9
- up_weight: float32 [2048, 8192], P('fs', 'tp'), may hold values from -0.125 to 0.125
- up_scale: float32 [8192], P('tp'), may hold values from 0.5 to 2
- down_weight: float32 [8192, 2048], P('tp', 'fs'), may hold values from -0.0625 to 0.0625
- down_scale: float32 [2048], P('fs'), may hold values from 0.5 to 2
Outputs:
- output: bfloat16 [49152, 2048], P('fs', 'tp')
All inputs are finite; a program needn't handle non-finite values.
Results may differ from a plain program's by a relative error of at most 0.015.
Values may be sent and summed in bfloat16 or wider, within the bound.
No kernel may reach another device: no remote copies, remote signals or barrier semaphores. Data moves between devices by JAX's collectives and lax.ppermute only.
A program may use at most 64 MiB of HBM per device.

v0:
```python
import jax
import jax.numpy as jnp
from jax import lax
from jax.sharding import Mesh
from jax.sharding import PartitionSpec as P

FS = ("fs_0", "fs_1")
epsilon = 1e-06


def cut_along(array, dim, count):
    before, after = (array.shape[:dim], array.shape[dim + 1 :])
    return jnp.moveaxis(array.reshape(*before, count, -1, *after), dim, 0)


def summed_on_arrival(array, axis, dim):
    count = lax.axis_size(axis)
    tiles = lax.all_to_all(cut_along(array, dim, count), axis, 0, 0, tiled=True)
    return jnp.sum(tiles.astype(jnp.float32), axis=0)


def local(tokens, norm_gain, up_weight, up_scale, down_weight, down_scale):
    up_half = up_weight.astype(jnp.bfloat16)
    down_rows = (down_weight.T * down_scale[:, None]).astype(jnp.bfloat16)
    up_whole = lax.all_gather(up_half, FS, axis=0, tiled=True)
    down_whole = lax.all_gather(down_rows, FS, axis=0, tiled=True)
    floats = tokens.astype(jnp.float32)
    inverse = lax.rsqrt(jnp.mean(floats * floats, axis=-1, keepdims=True) + epsilon)
    normed = (floats * inverse * norm_gain).astype(jnp.bfloat16)
    up_pre = jnp.dot(normed, up_whole, preferred_element_type=jnp.float32)
    hidden = jnp.square(jax.nn.relu(up_pre * up_scale)).astype(jnp.bfloat16)
    hidden = lax.optimization_barrier(hidden)
    partial_value = lax.dot_general(
        hidden, down_whole, (((1,), (1,)), ((), ())), preferred_element_type=jnp.float32
    ).astype(jnp.bfloat16)
    return summed_on_arrival(partial_value, "tp", 1).astype(jnp.bfloat16)


def solution(mesh):
    split = Mesh(mesh.devices.reshape(16, 4, mesh.shape["tp"]), ("fs_0", "fs_1", "tp"))
    return jax.shard_map(
        local,
        mesh=split,
        in_specs=(P(FS, None), P(), P(FS, "tp"), P("tp"), P("tp", FS), P(FS)),
        out_specs=P(FS, "tp"),
        check_vma=False,
    )
```

profile of v0, /device:TPU:1, one launch (start us, length us, event | category | flops | bytes accessed | tf_op | source)
XLA Modules:
  0.0 362.0 jit_solution(8417288208690118681)
XLA Ops:
  6.5 0.0 copy-start
  6.5 0.0 copy-start.2
  6.5 0.0 copy-start.1
  6.5 0.0 all-gather.3.cloned.1.call-start
  6.5 1.7 convert_element_type.25
  8.2 0.0 all-gather.3.cloned.1.call-update
  8.3 0.0 all-gather.5.cloned.1.call-start
  8.3 1.6 fusion.9
  9.9 0.0 all-gather.5.cloned.1.call-update
  9.9 2.6 fusion
  12.5 140.0 %all-gather.3.cloned.1.call-done = bf16[2048,1024]{1,0:T(8,128)(2,1)} async-done(((bf16[32,1024]{1,0:T(8,128)(2,1)}), bf16[2048,1024]{1,0:T(8,128)(2,1)}) %all-gather.3.cloned.1.call-update) | async-done | bytes 4194320 | tf_op jit(solution)/shard_map/all_gather | solution.py:25
  152.5 0.0 copy-done
  152.5 0.0 copy-done.2
  152.5 0.0 copy-done.1
  152.6 6.9 %multiply_convert_fusion = bf16[768,1024]{1,0:T(8,128)(2,1)} fusion(bf16[2048,1024]{1,0:T(8,128)(2,1)} %all-gather.3.cloned.1.call-done, bf16[768,2048]{1,0:T(8,128)(2,1)S(1)} %copy-done, f32[2048]{0:T(1024)S(1)} %copy-done.1, f32[768]{0:T(1024)S(1)} %add_rsqrt_fusion, f32[1024]{0:T(1024)S(1)} %copy-done.2), kind=kOutput, calls=%fused_computation.8 | convolution fusion | flops 3230662656 | bytes 8928256 | tf_op jit(solution)/shard_map/dot_general | solution.py:30
  159.4 137.0 %all-gather.5.cloned.1.call-done = bf16[2048,1024]{1,0:T(8,128)(2,1)} async-done(((bf16[32,1024]{1,0:T(8,128)(2,1)}), bf16[2048,1024]{1,0:T(8,128)(2,1)}) %all-gather.5.cloned.1.call-update) | async-done | bytes 4194320 | tf_op jit(solution)/shard_map/all_gather | solution.py:26
  296.4 6.1 %convolution_convert_fusion = bf16[768,2048]{1,0:T(8,128)(2,1)S(1)} fusion(bf16[768,1024]{1,0:T(8,128)(2,1)} %multiply_convert_fusion, bf16[2048,1024]{1,0:T(8,128)(2,1)} %all-gather.5.cloned.1.call-done), kind=kOutput, calls=%fused_computation.5 | convolution fusion | flops 3222798336 | bytes 8912896 | tf_op jit(solution)/shard_map/dot_general | solution.py:33
  302.5 0.2 copy.10
  302.8 51.1 %all_to_all.5 = bf16[8,768,256]{2,1,0:T(8,128)(2,1)S(1)} all-to-all(bf16[8,768,256]{2,1,0:T(8,128)(2,1)S(1)} %bitcast.12), channel_id=1, replica_groups=mesh['fs_0'=16,'fs_1'=4,'tp'=8] {'tp'}, dimensions={0} | all-to-all | bytes 6291456 | tf_op jit(solution)/shard_map/all_to_all | solution.py:18
  353.9 1.3 reduce_sum.22
  (1 shorter events, 0.0 us)
Async XLA Ops:
  6.5 146.0 %copy-start = (bf16[768,2048]{1,0:T(8,128)(2,1)S(1)}, bf16[768,2048]{1,0:T(8,128)(2,1)}, u32[]{:S(2)}) copy-start(bf16[768,2048]{1,0:T(8,128)(2,1)} %param.6) | copy-start | bytes 9437188
  6.5 146.0 %copy-start.2 = (f32[1024]{0:T(1024)S(1)}, f32[1024]{0:T(1024)}, u32[]{:S(2)}) copy-start(f32[1024]{0:T(1024)} %param.9) | copy-start | bytes 12292
  6.5 146.0 %copy-start.1 = (f32[2048]{0:T(1024)S(1)}, f32[2048]{0:T(1024)}, u32[]{:S(2)}) copy-start(f32[2048]{0:T(1024)} %param.7) | copy-start | bytes 24580
  6.5 146.0 %all-gather.3.cloned.1.call-start = ((), (), s32[]{:S(2)}) async-start(), calls=%async_computation.1 | async-start | bytes 4259840 | tf_op jit(solution)/shard_map/all_gather | solution.py:25
  8.3 288.2 %all-gather.5.cloned.1.call-start = ((), (), s32[]{:S(2)}) async-start(), calls=%async_computation.2 | async-start | bytes 4259840 | tf_op jit(solution)/shard_map/all_gather | solution.py:26
Sparse Core Ops, SparseCore 0:
  10.3 142.2 all-gather.2
  155.5 140.8 all-gather.4
where the time goes:
time: 362 us
  waiting for transfers between devices  277 us (77%)
  blocking collectives  51.1 us (14%)
  between operations  13.4 us (4%)
  matrix products  13 us (4%)
  other arithmetic  7.15 us (2%)
    all_gather x1, waiting for transfers between devices, local(): up_whole = lax.all_gather(up_half, FS, axis=0, tiled=True)  140 us
    all_gather x1, waiting for transfers between devices, local(): down_whole = lax.all_gather(down_rows, FS, axis=0, tiled=True)  137 us
    all_to_all x1, blocking collectives, summed_on_arrival(): tiles = lax.all_to_all(cut_along(array, dim, count), axis, 0, 0, tiled=True)  51.1 us
  transfers between devices with their start and end apart: 2, of which 2 were waited for; matrix products, arithmetic and copies ran while one was open for 3% of the time, Pallas kernels for 0%

commit v1 on v0

--- a/solution.py
+++ b/solution.py
@@ -22,8 +22,11 @@
 def local(tokens, norm_gain, up_weight, up_scale, down_weight, down_scale):
     up_half = up_weight.astype(jnp.bfloat16)
     down_rows = (down_weight.T * down_scale[:, None]).astype(jnp.bfloat16)
-    up_whole = lax.all_gather(up_half, FS, axis=0, tiled=True)
-    down_whole = lax.all_gather(down_rows, FS, axis=0, tiled=True)
+    up_whole, down_whole = jnp.split(
+        lax.all_gather(jnp.concatenate([up_half, down_rows], axis=1), FS, axis=0, tiled=True),
+        [up_half.shape[1]],
+        axis=1,
+    )
     floats = tokens.astype(jnp.float32)
     inverse = lax.rsqrt(jnp.mean(floats * floats, axis=-1, keepdims=True) + epsilon)
     normed = (floats * inverse * norm_gain).astype(jnp.bfloat16)

time: 362 us -> 232 us (0.64)
  waiting for transfers between devices: 277 us -> 152 us
    all_gather x2 -> x1, waiting for transfers between devices: 277 us -> 152 us  [local(): lax.all_gather(jnp.concatenate([up_half, down_rows], axis=1), FS, axis=0,...]
  transfers between devices with their start and end apart: 2 -> 1, of which waited for: 2 -> 1; matrix products, arithmetic and copies ran while one was open for 3% -> 1% of each run, Pallas kernels for 0% -> 0%
where the time goes in v1:
time: 232 us
  waiting for transfers between devices  152 us (66%)
  blocking collectives  49.9 us (22%)
  between operations  13.4 us (6%)
  matrix products  9.51 us (4%)
  other arithmetic  6.57 us (3%)
    all_gather x1, waiting for transfers between devices, local(): lax.all_gather(jnp.concatenate([up_half, down_rows], axis=1), FS, axis=0,...  152 us
    all_to_all x1, blocking collectives, summed_on_arrival(): tiles = lax.all_to_all(cut_along(array, dim, count), axis, 0, 0, tiled=True)  49.9 us
    dot_general x1, matrix products, local(): up_pre = jnp.dot(normed, up_whole, preferred_element_type=jnp.float32)  5.8 us
  transfers between devices with their start and end apart: 1, of which 1 were waited for; matrix products, arithmetic and copies ran while one was open for 1% of the time, Pallas kernels for 0%

profile of v1, /device:TPU:1, one launch (start us, length us, event | category | flops | bytes accessed | tf_op | source)
XLA Modules:
  0.0 231.7 jit_solution(5611939754312704504)
XLA Ops:
  6.5 0.0 copy-start
  6.5 0.0 copy-start.3
  6.5 0.0 copy-start.2
  6.5 0.0 all-gather.2.cloned.1.call-start
  6.5 1.1 convert_element_type.25
  7.6 1.0 fusion.17
  8.6 0.7 pad_maximum_fusion
  9.3 0.0 all-gather.2.cloned.1.call-update
  9.3 2.6 %fusion = f32[768]{0:T(1024)S(1)} fusion(bf16[768,2048]{1,0:T(8,128)(2,1)} %param.6), kind=kLoop, calls=%fused_computation.2 | loop fusion | flops 4717824 | bytes 3148800 | tf_op jit(solution)/shard_map/reduce_sum | solution.py:31
  11.9 152.1 %all-gather.2.cloned.1.call-done = bf16[2048,2048]{1,0:T(8,128)(2,1)} async-done(((bf16[32,2048]{1,0:T(8,128)(2,1)}), bf16[2048,2048]{1,0:T(8,128)(2,1)}) %all-gather.2.cloned.1.call-update) | async-done | bytes 8388624 | tf_op jit(solution)/shard_map/all_gather | solution.py:26
  164.0 0.0 copy-done
  164.0 0.0 copy-done.3
  164.0 0.0 copy-done.2
  164.0 0.0 copy-start.1
  164.0 5.8 %multiply_convert_fusion = bf16[768,1024]{1,0:T(8,128)(2,1)S(1)} fusion(bf16[2048,2048]{1,0:T(8,128)(2,1)} %all-gather.2.cloned.1.call-done, bf16[768,2048]{1,0:T(8,128)(2,1)S(1)} %copy-done, f32[2048]{0:T(1024)S(1)} %copy-done.2, f32[768]{0:T(1024)S(1)} %add_rsqrt_fusion, f32[1024]{0:T(1024)S(1)} %copy-done.3), kind=kOutput, calls=%fused_computation.11 | convolution fusion | flops 3230662656 | bytes 8928256 | tf_op jit(solution)/shard_map/dot_general | solution.py:33
  169.8 0.0 copy-done.1
  169.8 3.7 %fusion.7 = bf16[768,2048]{1,0:T(8,128)(2,1)S(1)} fusion(bf16[768,1024]{1,0:T(8,128)(2,1)S(1)} %multiply_convert_fusion, bf16[2048,2048]{1,0:T(8,128)(2,1)S(1)} %copy-done.1), kind=kOutput, calls=%fused_computation.9 | convolution fusion | flops 3222798336 | bytes 8912896 | tf_op jit(solution)/shard_map/dot_general | solution.py:36
  173.5 0.2 copy.10
  173.7 49.9 %all_to_all.5 = bf16[8,768,256]{2,1,0:T(8,128)(2,1)S(1)} all-to-all(bf16[8,768,256]{2,1,0:T(8,128)(2,1)S(1)} %bitcast.10), channel_id=1, replica_groups=mesh['fs_0'=16,'fs_1'=4,'tp'=8] {'tp'}, dimensions={0} | all-to-all | bytes 6291456 | tf_op jit(solution)/shard_map/all_to_all | solution.py:18
  223.6 1.3 reduce_sum.22
  (1 shorter events, 0.0 us)
Async XLA Ops:
  6.5 157.4 %copy-start = (bf16[768,2048]{1,0:T(8,128)(2,1)S(1)}, bf16[768,2048]{1,0:T(8,128)(2,1)}, u32[]{:S(2)}) copy-start(bf16[768,2048]{1,0:T(8,128)(2,1)} %param.6) | copy-start | bytes 9437188
  6.5 157.4 %copy-start.3 = (f32[1024]{0:T(1024)S(1)}, f32[1024]{0:T(1024)}, u32[]{:S(2)}) copy-start(f32[1024]{0:T(1024)} %param.9) | copy-start | bytes 12292
  6.5 157.4 %copy-start.2 = (f32[2048]{0:T(1024)S(1)}, f32[2048]{0:T(1024)}, u32[]{:S(2)}) copy-start(f32[2048]{0:T(1024)} %param.7) | copy-start | bytes 24580
  6.5 157.4 %all-gather.2.cloned.1.call-start = ((), (), s32[]{:S(2)}) async-start(), calls=%async_computation.1 | async-start | bytes 8519680 | tf_op jit(solution)/shard_map/all_gather | solution.py:26
  164.0 5.8 %copy-start.1 = (bf16[2048,2048]{1,0:T(8,128)(2,1)S(1)}, bf16[2048,2048]{1,0:T(8,128)(2,1)}, u32[]{:S(2)}) copy-start(bf16[2048,2048]{1,0:T(8,128)(2,1)} %all-gather.2.cloned.1.call-done) | copy-start | bytes 25165828
Sparse Core Ops, SparseCore 0:
  10.3 153.6 all-gather.1

commit v2 on v0

--- a/solution.py
+++ b/solution.py
@@ -22,7 +22,9 @@
 def local(tokens, norm_gain, up_weight, up_scale, down_weight, down_scale):
     up_half = up_weight.astype(jnp.bfloat16)
     down_rows = (down_weight.T * down_scale[:, None]).astype(jnp.bfloat16)
-    up_whole = lax.all_gather(up_half, FS, axis=0, tiled=True)
+    up_whole = jnp.concatenate(
+        lax.all_to_all(jnp.stack([up_half] * lax.axis_size(FS)), FS, 0, 0), axis=0
+    )
     down_whole = lax.all_gather(down_rows, FS, axis=0, tiled=True)
     floats = tokens.astype(jnp.float32)
     inverse = lax.rsqrt(jnp.mean(floats * floats, axis=-1, keepdims=True) + epsilon)

time: 362 us -> 307 us (0.85)
  waiting for transfers between devices: 277 us -> 205 us
  starting transfers between devices: 0.04 us -> 19.8 us
    all_to_all x0 -> x1, waiting for transfers between devices: none -> 205 us  [local(): lax.all_to_all(jnp.stack([up_half] * lax.axis_size(FS)), FS, 0, 0)]
    all_gather x1 -> x0, waiting for transfers between devices: 140 us -> none  [local(): up_whole = lax.all_gather(up_half, FS, axis=0, tiled=True)]
    all_gather x1, waiting for transfers between devices: 137 us -> 0.01 us  [local(): down_whole = lax.all_gather(down_rows, FS, axis=0, tiled=True)]
    all_to_all x0 -> x1, starting transfers between devices: none -> 19.8 us  [local(): lax.all_to_all(jnp.stack([up_half] * lax.axis_size(FS)), FS, 0, 0)]
  transfers between devices with their start and end apart: 2 -> 2, of which waited for: 2 -> 1; matrix products, arithmetic and copies ran while one was open for 3% -> 3% of each run, Pallas kernels for 0% -> 0%
where the time goes in v2:
time: 307 us
  waiting for transfers between devices  205 us (67%)
  blocking collectives  49.3 us (16%)
  starting transfers between devices  19.8 us (6%)
  between operations  13.5 us (4%)
  matrix products  13 us (4%)
  other arithmetic  3.59 us (1%)
    all_to_all x1, waiting for transfers between devices, local(): lax.all_to_all(jnp.stack([up_half] * lax.axis_size(FS)), FS, 0, 0)  205 us
    all_to_all x1, blocking collectives, summed_on_arrival(): tiles = lax.all_to_all(cut_along(array, dim, count), axis, 0, 0, tiled=True)  49.3 us
    all_to_all x1, starting transfers between devices, local(): lax.all_to_all(jnp.stack([up_half] * lax.axis_size(FS)), FS, 0, 0)  19.8 us
    dot_general x1, matrix products, local(): up_pre = jnp.dot(normed, up_whole, preferred_element_type=jnp.float32)  6.88 us
  transfers between devices with their start and end apart: 2, of which 1 were waited for; matrix products, arithmetic and copies ran while one was open for 3% of the time, Pallas kernels for 0%

profile of v2, /device:TPU:1, one launch (start us, length us, event | category | flops | bytes accessed | tf_op | source)
XLA Modules:
  0.0 306.6 jit_solution(12106306585804745655)
XLA Ops:
  6.5 0.9 convert_element_type.25
  7.4 2.5 stack.2
  9.9 0.0 copy-start.1
  9.9 0.0 copy-start.2
  9.9 0.0 copy-start
  9.9 19.8 %all-to-all-start = ((bf16[64,32,1024]{2,1,0:T(8,128)(2,1)}), bf16[64,32,1024]{2,1,0:T(8,128)(2,1)}, u32[]{:S(2)}, u32[]{:S(2)}) async-start(bf16[64,32,1024]{2,1,0:T(8,128)(2,1)} %stack.2), calls=%async_computation | async-start | bytes 8388608 | tf_op jit(solution)/shard_map/all_to_all | solution.py:26
  29.7 0.0 copy-start.3
  29.7 0.0 copy-start.4
  29.8 0.0 all-gather.2.cloned.1.call-start
  29.8 0.0 copy-done.1
  29.8 0.0 copy-done.2
  29.8 0.7 fusion.9
  30.5 0.0 all-gather.2.cloned.1.call-update
  30.6 0.0 copy-done
  30.6 0.7 fusion
  31.3 204.7 %all-to-all-done = bf16[64,32,1024]{2,1,0:T(8,128)(2,1)} async-done(((bf16[64,32,1024]{2,1,0:T(8,128)(2,1)}), bf16[64,32,1024]{2,1,0:T(8,128)(2,1)}, u32[]{:S(2)}, u32[]{:S(2)}) %all-to-all-start) | async-done | bytes 4194336 | tf_op jit(solution)/shard_map/all_to_all | solution.py:26
  236.0 0.0 copy-done.3
  236.0 0.0 copy-done.4
  236.0 6.9 %multiply_convert_fusion = bf16[768,1024]{1,0:T(8,128)(2,1)} fusion(bf16[2048,1024]{1,0:T(8,128)(2,1)} %bitcast, bf16[768,2048]{1,0:T(8,128)(2,1)S(1)} %copy-done, f32[2048]{0:T(1024)S(1)} %copy-done.3, f32[768]{0:T(1024)S(1)} %add_rsqrt_fusion, f32[1024]{0:T(1024)S(1)} %copy-done.4), kind=kOutput, calls=%fused_computation.8 | convolution fusion | flops 3230662656 | bytes 8928256 | tf_op jit(solution)/shard_map/dot_general | solution.py:32
  242.9 0.0 all-gather.2.cloned.1.call-done
  242.9 6.1 %convolution_convert_fusion = bf16[768,2048]{1,0:T(8,128)(2,1)S(1)} fusion(bf16[768,1024]{1,0:T(8,128)(2,1)} %multiply_convert_fusion, bf16[2048,1024]{1,0:T(8,128)(2,1)} %all-gather.2.cloned.1.call-done), kind=kOutput, calls=%fused_computation.5 | convolution fusion | flops 3222798336 | bytes 8912896 | tf_op jit(solution)/shard_map/dot_general | solution.py:35
  249.0 0.2 copy.10
  249.2 49.3 %all_to_all.10 = bf16[8,768,256]{2,1,0:T(8,128)(2,1)S(1)} all-to-all(bf16[8,768,256]{2,1,0:T(8,128)(2,1)S(1)} %bitcast.13), channel_id=1, replica_groups=mesh['fs_0'=16,'fs_1'=4,'tp'=8] {'tp'}, dimensions={0} | all-to-all | bytes 6291456 | tf_op jit(solution)/shard_map/all_to_all | solution.py:18
  298.5 1.3 reduce_sum.22
  (1 shorter events, 0.0 us)
Async XLA Ops:
  9.9 19.9 %copy-start.1 = (f32[1024,32]{0,1:T(8,128)S(1)}, f32[1024,32]{0,1:T(8,128)}, u32[]{:S(2)}) copy-start(f32[1024,32]{0,1:T(8,128)} %param.10) | copy-start | bytes 393220
  9.9 19.9 %copy-start.2 = (f32[32]{0:T(128)S(1)}, f32[32]{0:T(128)}, u32[]{:S(2)}) copy-start(f32[32]{0:T(128)} %param.11) | copy-start | bytes 388
  9.9 20.6 %copy-start = (bf16[768,2048]{1,0:T(8,128)(2,1)S(1)}, bf16[768,2048]{1,0:T(8,128)(2,1)}, u32[]{:S(2)}) copy-start(bf16[768,2048]{1,0:T(8,128)(2,1)} %param.6) | copy-start | bytes 9437188
  9.9 226.0 %all-to-all-start = ((bf16[64,32,1024]{2,1,0:T(8,128)(2,1)}), bf16[64,32,1024]{2,1,0:T(8,128)(2,1)}, u32[]{:S(2)}, u32[]{:S(2)}) async-start(bf16[64,32,1024]{2,1,0:T(8,128)(2,1)} %stack.2), calls=%async_computation | async-start | bytes 8388608 | tf_op jit(solution)/shard_map/all_to_all | solution.py:26
  29.7 206.2 %copy-start.3 = (f32[2048]{0:T(1024)S(1)}, f32[2048]{0:T(1024)}, u32[]{:S(2)}) copy-start(f32[2048]{0:T(1024)} %param.7) | copy-start | bytes 24580
  29.7 206.2 %copy-start.4 = (f32[1024]{0:T(1024)S(1)}, f32[1024]{0:T(1024)}, u32[]{:S(2)}) copy-start(f32[1024]{0:T(1024)} %param.9) | copy-start | bytes 12292
  29.8 213.1 %all-gather.2.cloned.1.call-start = ((), (), s32[]{:S(2)}) async-start(), calls=%async_computation.2 | async-start | bytes 4259840 | tf_op jit(solution)/shard_map/all_gather | solution.py:28
Sparse Core Ops, SparseCore 0:
  33.5 208.8 all-gather.1
